TPU v7x, 256 devices: a whole 4x4x8 slice. The times are simulated.
256 devices in a mesh: fs: 32 (over z, x), tp: 8 (over y, core).
Axes of the slice: x: 4, y: 4, z: 8, core: 2. Of those that a mesh axis runs over, the one named last changes fastest.
Arguments:
- tokens: bfloat16 [32768, 2048], P(('fs', 'tp')), may hold values from -6 to 6
- gate_pre: bfloat16 [32768, 5632], P('fs', 'tp'), may hold values from -6 to 6
- value_pre: bfloat16 [32768, 5632], P('fs', 'tp'), may hold values from -6 to 6
- up_gate_w: bfloat16 [2048, 5632], P('fs', 'tp'), may hold values from -0.078125 to 0.078125
- up_value_w: bfloat16 [2048, 5632], P('fs', 'tp'), may hold values from -0.078125 to 0.078125
- conv_weight: float32 [3, 5632], P(None, 'tp'), may hold values from -3 to 3
- conv_bias: float32 [5632], P('tp'), may hold values from -3 to 3
- hidden_grad: bfloat16 [32768, 5632], P('fs', 'tp'), may hold values from -6 to 6
Outputs:
- input_grad: bfloat16 [32768, 2048], P(('fs', 'tp'))
- up_gate_grad: float32 [2048, 5632], P('fs', 'tp')
- up_value_grad: float32 [2048, 5632], P('fs', 'tp')
- conv_weight_grad: float32 [3, 5632], P(None, 'tp')
- conv_bias_grad: float32 [5632], P('tp')
All inputs are finite; a program needn't handle non-finite values.
Results may differ from a plain program's by a relative error of at most 0.013.
Values may be sent and summed in bfloat16 or wider, within the bound.
No kernel may reach another device: no remote copies, remote signals or barrier semaphores. Data moves between devices by JAX's collectives and lax.ppermute only.
A program may use at most 128 MiB of HBM per device.

v0:
```python
import jax
import jax.numpy as jnp
from jax import lax
from jax.sharding import Mesh
from jax.sharding import PartitionSpec as P

FS = ("fs_0", "fs_1")
FS_TP = ("fs_0", "fs_1", "tp")


def copy_for_each(shard, axis):
    peers = lax.axis_size(axis)
    return lax.all_to_all(
        jnp.broadcast_to(shard[None], (peers, *shard.shape)), axis, 0, 0, tiled=True
    )


def taken_together(shard, axis):
    return copy_for_each(shard, axis).sum(axis=0)


def in_one_piece(arrays, axis, dim, along):
    ends, at = ([], 0)
    for a in arrays[:-1]:
        at += a.shape[along]
        ends.append(at)
    both = jnp.concatenate(arrays, axis=along)
    return tuple(jnp.split(lax.all_gather(both, axis, axis=dim, tiled=True), ends, axis=along))


def summed_rows(subtotal, axes):
    for axis in axes:
        subtotal = lax.psum_scatter(subtotal, axis, scatter_dimension=0, tiled=True)
    return subtotal


def in_blocks(shard, dim, peers):
    lengths = shard.shape
    blocks = shard.reshape(*lengths[:dim], peers, lengths[dim] // peers, *lengths[dim + 1 :])
    return jnp.moveaxis(blocks, dim, 0)


def summed_on_arrival(shard, axis, dim):
    blocks = in_blocks(shard, dim, lax.axis_size(axis))
    arrived = lax.all_to_all(blocks, axis, split_axis=0, concat_axis=0, tiled=True)
    return arrived.astype(jnp.float32).sum(axis=0)


def contract_rows(left, right):
    return lax.dot_general(
        left, right, (((0,), (0,)), ((), ())), preferred_element_type=jnp.float32
    )


def contract_cols(left, right):
    return lax.dot_general(
        left, right, (((1,), (1,)), ((), ())), preferred_element_type=jnp.float32
    )


def on_device(
    tokens, gate_pre, value_pre, up_gate_w, up_value_w, conv_weight, conv_bias, hidden_grad
):
    length = gate_pre.shape[0]
    col_count = gate_pre.shape[1]
    scale = float(length * lax.axis_size(FS)) ** (-0.5)
    gate_float = gate_pre.astype(jnp.float32)
    padded = jnp.pad(gate_float, ((2, 0), (0, 0)))
    gate_conv = (
        conv_bias
        + conv_weight[0] * padded[:length]
        + conv_weight[1] * padded[1 : length + 1]
        + conv_weight[2] * padded[2:]
    )
    active, gelu_back = jax.vjp(jax.nn.gelu, gate_conv)
    grad_float = hidden_grad.astype(jnp.float32)
    value_grad = (grad_float * active).astype(jnp.bfloat16)
    conv_grad = gelu_back(grad_float * value_pre.astype(jnp.float32))[0]
    shifted = jnp.pad(conv_grad, ((0, 2), (0, 0)))
    gate_grad = (
        conv_weight[2] * conv_grad
        + conv_weight[1] * shifted[1 : length + 1]
        + conv_weight[0] * shifted[2:]
    ).astype(jnp.bfloat16)
    conv_terms = jnp.stack(
        [
            jnp.sum(conv_grad * padded[:length], axis=0),
            jnp.sum(conv_grad * padded[1 : length + 1], axis=0),
            jnp.sum(conv_grad * padded[2:], axis=0),
            jnp.sum(conv_grad, axis=0),
        ]
    )
    conv_total = taken_together(conv_terms, FS) * scale
    whole_tokens = lax.all_gather(tokens, "tp", axis=0, tiled=True)
    full_gate, full_value = in_one_piece((up_gate_w, up_value_w), FS, 0, 1)
    joined = summed_rows(
        jnp.concatenate(
            [contract_rows(whole_tokens, gate_grad), contract_rows(whole_tokens, value_grad)],
            axis=1,
        ),
        FS,
    )
    gate_out = joined[:, :col_count] * scale
    value_out = joined[:, col_count:] * scale
    input_grad = summed_on_arrival(
        (contract_cols(gate_grad, full_gate) + contract_cols(value_grad, full_value)).astype(
            jnp.bfloat16
        ),
        "tp",
        0,
    ).astype(jnp.bfloat16)
    return (input_grad, gate_out, value_out, conv_total[:3], conv_total[3])


def solution(mesh):
    finer = Mesh(mesh.devices.reshape(8, 4, mesh.shape["tp"]), ("fs_0", "fs_1", "tp"))
    in_specs = (
        P(FS_TP, None),
        P(FS, "tp"),
        P(FS, "tp"),
        P(FS, "tp"),
        P(FS, "tp"),
        P(None, "tp"),
        P("tp"),
        P(FS, "tp"),
    )
    out_specs = (P(FS_TP, None), P(FS, "tp"), P(FS, "tp"), P(None, "tp"), P("tp"))
    return jax.shard_map(
        on_device, mesh=finer, in_specs=in_specs, out_specs=out_specs, check_vma=False
    )
```

profile of v0, /device:TPU:8, one launch (start us, length us, event | category | flops | bytes accessed | tf_op | source)
XLA Modules:
  0.0 301.7 jit_solution(17411305977214108581)
XLA Ops:
  7.2 0.0 all-gather.5.cloned.1.call-start
  7.3 0.7 all-gather.5.cloned.1.call-update
  7.9 0.0 all-gather.3.cloned.1.call-start
  8.0 1.8 pad_maximum_fusion.1
  9.8 0.0 all-gather.3.cloned.1.call-update
  9.8 0.0 reduce-scatter.5.cloned.1.call-start
  9.9 1.8 convert_element_type.26
  11.8 6.5 %multiply_reduce_fusion.2 = (f32[704]{0:T(1024)S(1)}, f32[704]{0:T(1024)S(1)}, f32[704]{0:T(1024)S(1)}, f32[704]{0:T(1024)S(1)}, f32[1024,704]{0,1:T(8,128)S(1)}, /*index=5*/f32[1024,704]{0,1:T(8,128)}) fusion(f32[1024,704]{0,1:T(8,128)S(1)} %convert_element_type.26, bf16[1024,704]{0,1:T(8,128)(2,1)S(1)} %copy-done, bf16[1024,704]{0,1:T(8,128)(2,1)S(1)} %copy-done.2, ...), kind=kLoop, calls=%fused_computation.29 | loop fusion | flops 25949440 | bytes 12998656 | tf_op jit(solution)/shard_map/reduce_sum | solution.py:87
  18.3 3.0 %fusion.6 = bf16[1024,704]{0,1:T(8,128)(2,1)} fusion(f32[1024,704]{0,1:T(8,128)S(1)} %get-tuple-element.32, f32[704]{0:T(1024)S(1)} %get-tuple-element.30, f32[704]{0:T(1024)S(1)} %get-tuple-element.31, f32[704]{0:T(1024)S(1)} %get-tuple-element.29), kind=kLoop, calls=%fused_computation.18 | loop fusion | flops 4325376 | bytes 4333824 | tf_op jit(solution)/shard_map/convert_element_type | solution.py:84
  21.4 25.0 %all-gather.5.cloned.1.call-done = bf16[1024,2048]{1,0:T(8,128)(2,1)} async-done(((bf16[128,2048]{1,0:T(8,128)(2,1)}), bf16[1024,2048]{1,0:T(8,128)(2,1)}) %all-gather.5.cloned.1.call-update) | async-done | bytes 4194320 | tf_op jit(solution)/shard_map/all_gather | solution.py:94
  46.4 8.4 %convolution_bitcast_fusion.1 = f32[2048,704]{0,1:T(8,128)} fusion(bf16[1024,704]{0,1:T(8,128)(2,1)} %fusion.6, bf16[1024,2048]{1,0:T(8,128)(2,1)} %all-gather.5.cloned.1.call-done), kind=kOutput, calls=%fused_computation.5 | convolution fusion | flops 2952790016 | bytes 11403264 | tf_op jit(solution)/shard_map/dot_general | solution.py:50
  54.8 5.3 %convolution_bitcast_fusion = f32[2048,704]{0,1:T(8,128)} fusion(bf16[1024,2048]{1,0:T(8,128)(2,1)S(1)} %copy-done.10, bf16[1024,704]{0,1:T(8,128)(2,1)S(1)} %copy-done.4, f32[1024,704]{0,1:T(8,128)S(1)} %copy-done.1), kind=kOutput, calls=%fused_computation.4 | convolution fusion | flops 2960719872 | bytes 14286848 | tf_op jit(solution)/shard_map/dot_general | solution.py:50
  60.1 10.8 %pad_maximum_fusion = f32[2048,1408]{0,1:T(8,128)} fusion(f32[2048,704]{0,1:T(8,128)} %convolution_bitcast_fusion, f32[2048,704]{0,1:T(8,128)} %convolution_bitcast_fusion.1), kind=kLoop, calls=%fused_computation | loop fusion | flops 2883584 | bytes 23068672 | tf_op jit(solution)/shard_map/concatenate | solution.py:97
  70.9 0.0 reduce-scatter.5.cloned.1.call-update
  71.0 0.8 broadcast_in_dim.2
  71.8 10.0 %all-to-all-start.1 = ((f32[32,4,704]{2,1,0:T(4,128)}), f32[32,4,704]{2,1,0:T(4,128)S(1)}, u32[]{:S(2)}, u32[]{:S(2)}) async-start(f32[32,4,704]{2,1,0:T(4,128)} %broadcast_in_dim.2), calls=%async_computation.2 | async-start | bytes 786432 | tf_op jit(solution)/shard_map/all_to_all | solution.py:13
  81.8 56.8 %all-gather.3.cloned.1.call-done = bf16[2048,1408]{1,0:T(8,128)(2,1)} async-done(((bf16[64,1408]{1,0:T(8,128)(2,1)}), bf16[2048,1408]{1,0:T(8,128)(2,1)}) %all-gather.3.cloned.1.call-update) | async-done | bytes 5767184 | tf_op jit(solution)/shard_map/all_gather | solution.py:28
  138.7 6.0 %fusion.1 = f32[1024,2048]{1,0:T(8,128)S(1)} fusion(bf16[1024,704]{0,1:T(8,128)(2,1)} %fusion.6, bf16[2048,1408]{1,0:T(8,128)(2,1)} %all-gather.3.cloned.1.call-done), kind=kOutput, calls=%fused_computation.13 | convolution fusion | flops 2952790016 | bytes 12976128 | tf_op jit(solution)/shard_map/dot_general | solution.py:56
  144.7 7.6 %add_convert_fusion = bf16[1024,2048]{1,0:T(8,128)(2,1)} fusion(f32[1024,2048]{1,0:T(8,128)S(1)} %fusion.1, bf16[2048,1408]{1,0:T(8,128)(2,1)S(1)} %copy-done.9, bf16[1024,704]{0,1:T(8,128)(2,1)S(1)} %copy-done.5, f32[1024,704]{0,1:T(8,128)S(1)} %copy-done.1), kind=kOutput, calls=%fused_computation.1 | convolution fusion | flops 2964914176 | bytes 20054016 | tf_op jit(solution)/shard_map/dot_general | solution.py:56
  152.3 5.0 %all-to-all-start = ((bf16[8,128,2048]{2,1,0:T(8,128)(2,1)}), bf16[8,128,2048]{2,1,0:T(8,128)(2,1)}, u32[]{:S(2)}, u32[]{:S(2)}) async-start(bf16[8,128,2048]{2,1,0:T(8,128)(2,1)} %bitcast.11), calls=%async_computation | async-start | bytes 8388608 | tf_op jit(solution)/shard_map/all_to_all | solution.py:45
  157.3 105.4 %reduce-scatter.5.cloned.1.call-done = f32[256,1408]{0,1:T(8,128)} async-done(((f32[2048,1408]{0,1:T(8,128)}), f32[256,1408]{0,1:T(8,128)}) %reduce-scatter.5.cloned.1.call-update) | async-done | bytes 1441808 | tf_op jit(solution)/shard_map/reduce_scatter | solution.py:33
  262.6 2.9 copy.22
  265.5 0.0 reduce-scatter.7.cloned.1.call-update
  265.6 0.1 reduce_sum.62
  265.7 0.6 slice_reduce_fusion
  266.3 3.8 %reduce_sum.57 = bf16[128,2048]{1,0:T(8,128)(2,1)} reduce(bf16[8,128,2048]{2,1,0:T(8,128)(2,1)} %all-to-all-done, bf16[]{:T(256)} %constant.19.clone.1), dimensions={0}, to_apply=%region_0.1 | reduce | flops 1835008 | bytes 4718594 | tf_op jit(solution)/shard_map/reduce_sum | solution.py:46
  270.1 21.8 %reduce-scatter.7.cloned.1.call-done = f32[64,1408]{1,0:T(8,128)} async-done(((f32[256,1408]{1,0:T(8,128)}), f32[64,1408]{1,0:T(8,128)}) %reduce-scatter.7.cloned.1.call-update) | async-done | bytes 360464
  292.0 1.1 fusion.18
  293.1 0.2 copy.25
  293.3 0.8 copy.20
  294.1 0.2 copy.26
  294.3 0.8 copy.21
  (34 shorter events, 0.2 us)
Async XLA Ops:
  7.2 4.6 %copy-start = (bf16[1024,704]{0,1:T(8,128)(2,1)S(1)}, bf16[1024,704]{0,1:T(8,128)(2,1)}, u32[]{:S(2)}) copy-start(bf16[1024,704]{0,1:T(8,128)(2,1)} %param.9) | copy-start | bytes 4325380
  7.2 4.5 %copy-start.7 = (f32[3,704]{1,0:T(4,128)S(1)}, f32[3,704]{1,0:T(4,128)}, u32[]{:S(2)}) copy-start(f32[3,704]{1,0:T(4,128)} %param.13) | copy-start | bytes 25348
  7.2 4.6 %copy-start.2 = (bf16[1024,704]{0,1:T(8,128)(2,1)S(1)}, bf16[1024,704]{0,1:T(8,128)(2,1)}, u32[]{:S(2)}) copy-start(bf16[1024,704]{0,1:T(8,128)(2,1)} %param.10) | copy-start | bytes 4325380
  7.2 4.6 %copy-start.8 = (f32[704]{0:T(1024)S(1)}, f32[704]{0:T(1024)}, u32[]{:S(2)}) copy-start(f32[704]{0:T(1024)} %param.14) | copy-start | bytes 8452
  7.2 39.2 %all-gather.5.cloned.1.call-start = ((), (), s32[]{:S(2)}) async-start(), calls=%async_computation.5 | async-start | bytes 4718592 | tf_op jit(solution)/shard_map/all_gather | solution.py:94
  7.9 130.7 %all-gather.3.cloned.1.call-start = ((), (), s32[]{:S(2)}) async-start(), calls=%async_computation.4 | async-start | bytes 5947392 | tf_op jit(solution)/shard_map/all_gather | solution.py:28
  9.8 252.8 %reduce-scatter.5.cloned.1.call-start = ((), (), s32[]{:S(2)}) async-start(), calls=%async_computation.6 | async-start | bytes 12976128 | tf_op jit(solution)/shard_map/reduce_scatter | solution.py:33
  9.9 1.9 copy-start.3
  21.4 33.4 %copy-start.1 = (f32[1024,704]{0,1:T(8,128)S(1)}, f32[1024,704]{0,1:T(8,128)}, u32[]{:S(2)}) copy-start(f32[1024,704]{0,1:T(8,128)} %get-tuple-element.33) | copy-start | bytes 8650756
  46.4 8.4 %copy-start.4 = (bf16[1024,704]{0,1:T(8,128)(2,1)S(1)}, bf16[1024,704]{0,1:T(8,128)(2,1)}, u32[]{:S(2)}) copy-start(bf16[1024,704]{0,1:T(8,128)(2,1)} %param.15) | copy-start | bytes 4325380
  46.4 8.4 %copy-start.10 = (bf16[1024,2048]{1,0:T(8,128)(2,1)S(1)}, bf16[1024,2048]{1,0:T(8,128)(2,1)}, u32[]{:S(2)}) copy-start(bf16[1024,2048]{1,0:T(8,128)(2,1)} %all-gather.5.cloned.1.call-done) | copy-start | bytes 12582916
  71.8 80.4 %all-to-all-start.1 = ((f32[32,4,704]{2,1,0:T(4,128)}), f32[32,4,704]{2,1,0:T(4,128)S(1)}, u32[]{:S(2)}, u32[]{:S(2)}) async-start(f32[32,4,704]{2,1,0:T(4,128)} %broadcast_in_dim.2), calls=%async_computation.2 | async-start | bytes 786432 | tf_op jit(solution)/shard_map/all_to_all | solution.py:13
  138.7 6.0 %copy-start.5 = (bf16[1024,704]{0,1:T(8,128)(2,1)S(1)}, bf16[1024,704]{0,1:T(8,128)(2,1)}, u32[]{:S(2)}) copy-start(bf16[1024,704]{0,1:T(8,128)(2,1)} %param.15) | copy-start | bytes 4325380
  138.7 6.0 %copy-start.9 = (bf16[2048,1408]{1,0:T(8,128)(2,1)S(1)}, bf16[2048,1408]{1,0:T(8,128)(2,1)}, u32[]{:S(2)}) copy-start(bf16[2048,1408]{1,0:T(8,128)(2,1)} %all-gather.3.cloned.1.call-done) | copy-start | bytes 17301508
  152.3 114.0 %all-to-all-start = ((bf16[8,128,2048]{2,1,0:T(8,128)(2,1)}), bf16[8,128,2048]{2,1,0:T(8,128)(2,1)}, u32[]{:S(2)}, u32[]{:S(2)}) async-start(bf16[8,128,2048]{2,1,0:T(8,128)(2,1)} %bitcast.11), calls=%async_computation | async-start | bytes 8388608 | tf_op jit(solution)/shard_map/all_to_all | solution.py:45
  157.3 134.7 %reduce-scatter.7.cloned.1.call-start = ((), (), s32[]{:S(2)}) async-start(), calls=%async_computation.7 | async-start | bytes 1802240
  265.7 27.6 %copy-start.6 = (f32[4,704]{1,0:T(4,128)}, f32[4,704]{1,0:T(4,128)S(1)}, u32[]{:S(2)}) copy-start(f32[4,704]{1,0:T(4,128)S(1)} %broadcast_multiply_fusion.2) | copy-start | bytes 33796
Sparse Core Ops, SparseCore 0:
  9.9 36.4 all-gather.4
  49.5 89.0 all-gather.2
  141.2 121.3 reduce-scatter.4
  265.7 26.2 reduce-scatter.6
where the time goes:
time: 302 us
  waiting for transfers between devices  210 us (70%)
  other arithmetic  28 us (9%)
  matrix products  27.3 us (9%)
  starting transfers between devices  15.1 us (5%)
  between operations  14 us (5%)
  local copies, waits for them, and re-layouts  7.54 us (2%)
    reduce_scatter x1, waiting for transfers between devices, summed_rows(): subtotal = lax.psum_scatter(subtotal, axis, scatter_dimension=0, tiled=True)  105 us
    all_gather x1, waiting for transfers between devices, in_one_piece(): lax.all_gather(both, axis, axis=dim, tiled=True)  56.8 us
    all_gather x1, waiting for transfers between devices, on_device(): whole_tokens = lax.all_gather(tokens, 'tp', axis=0, tiled=True)  25 us
    unnamed x5, waiting for transfers between devices  22.5 us
    dot_general x2, matrix products, contract_rows(): lax.dot_general(left, right, (((0,), (0,)), ((), ())), preferred_element_...  13.7 us
    dot_general x2, matrix products, contract_cols(): lax.dot_general(left, right, (((1,), (1,)), ((), ())), preferred_element_...  13.6 us
    concatenate x1, other arithmetic, on_device(): jnp.concatenate([contract_rows(whole_tokens, gate_grad), contract_rows(wh...  10.8 us
    all_to_all x1, starting transfers between devices, copy_for_each(): lax.all_to_all(jnp.broadcast_to(shard[None], (peers, *shard.shape)), axis...  10 us
  transfers between devices with their start and end apart: 6, of which 4 were waited for; matrix products, arithmetic and copies ran while one was open for 20% of the time, Pallas kernels for 0%

commit v1 on v0

--- a/solution.py
+++ b/solution.py
@@ -3,6 +3,7 @@
 from jax import lax
 from jax.sharding import Mesh
 from jax.sharding import PartitionSpec as P
+from jax.lax import axis_index, axis_size, ppermute
 
 FS = ("fs_0", "fs_1")
 FS_TP = ("fs_0", "fs_1", "tp")
@@ -61,6 +62,21 @@
 def on_device(
     tokens, gate_pre, value_pre, up_gate_w, up_value_w, conv_weight, conv_bias, hidden_grad
 ):
+
+    def row_begin(xx, net_axis, dim_at):
+        cores_n = axis_size(net_axis)
+        bank = [(ix, (ix + 1) % cores_n) for ix in range(cores_n)]
+
+        def map_the_inputs(piece_next):
+            if len(piece_next) == cores_n:
+                return piece_next
+            return map_the_inputs(
+                [ppermute(piece_next[0], axis_name=net_axis, perm=bank), *piece_next]
+            )
+
+        b_now = jnp.concatenate(map_the_inputs([xx]), axis=dim_at)
+        return jnp.roll(b_now, (axis_index(net_axis) + 1) * xx.shape[dim_at], axis=dim_at)
+
     length = gate_pre.shape[0]
     col_count = gate_pre.shape[1]
     scale = float(length * lax.axis_size(FS)) ** (-0.5)
@@ -91,7 +107,7 @@
         ]
     )
     conv_total = taken_together(conv_terms, FS) * scale
-    whole_tokens = lax.all_gather(tokens, "tp", axis=0, tiled=True)
+    whole_tokens = row_begin(tokens, "tp", 0)
     full_gate, full_value = in_one_piece((up_gate_w, up_value_w), FS, 0, 1)
     joined = summed_rows(
         jnp.concatenate(

time: 302 us -> 277 us (0.917)
  waiting for transfers between devices: 210 us -> 172 us
  starting transfers between devices: 15.1 us -> 24.7 us
  local copies, waits for them, and re-layouts: 7.54 us -> 13 us
    all_gather x1, waiting for transfers between devices: 56.8 us -> 0.02 us  [in_one_piece(): lax.all_gather(both, axis, axis=dim, tiled=True)]
    ppermute x0 -> x7, waiting for transfers between devices: none -> 50.2 us  [map_the_inputs(): ppermute(piece_next[0], axis_name=net_axis, perm=bank)]
    all_gather x1 -> x0, waiting for transfers between devices: 25 us -> none  [on_device(): whole_tokens = lax.all_gather(tokens, 'tp', axis=0, tiled=True)]
    reduce_scatter x1, waiting for transfers between devices: 105 us -> 94 us  [summed_rows(): subtotal = lax.psum_scatter(subtotal, axis, scatter_dimension=0, tiled=True)]
    all_to_all x1, starting transfers between devices: 4.97 us -> 13 us  [summed_on_arrival(): lax.all_to_all(blocks, axis, split_axis=0, concat_axis=0, tiled=True)]
    unnamed x27 -> x60, local copies, waits for them, and re-layouts: 4.96 us -> 10.4 us
    unnamed x5 -> x4, waiting for transfers between devices: 22.5 us -> 25 us
  transfers between devices with their start and end apart: 6 -> 12, of which waited for: 4 -> 10; matrix products, arithmetic and copies ran while one was open for 20% -> 21% of each run, Pallas kernels for 0% -> 0%
where the time goes in v1:
time: 277 us; the launch traced here: 276 us
  waiting for transfers between devices  172 us (62%)
  other arithmetic  26.9 us (10%)
  starting transfers between devices  24.7 us (9%)
  matrix products  24.4 us (9%)
  between operations  16 us (6%)
  local copies, waits for them, and re-layouts  13 us (5%)
    reduce_scatter x1, waiting for transfers between devices, summed_rows(): subtotal = lax.psum_scatter(subtotal, axis, scatter_dimension=0, tiled=True)  94 us
    ppermute x7, waiting for transfers between devices, map_the_inputs(): ppermute(piece_next[0], axis_name=net_axis, perm=bank)  50.2 us
    unnamed x4, waiting for transfers between devices  25 us
    dot_general x2, matrix products, contract_cols(): lax.dot_general(left, right, (((1,), (1,)), ((), ())), preferred_element_...  13.6 us
    all_to_all x1, starting transfers between devices, summed_on_arrival(): lax.all_to_all(blocks, axis, split_axis=0, concat_axis=0, tiled=True)  13 us
    all_to_all x1, starting transfers between devices, copy_for_each(): lax.all_to_all(jnp.broadcast_to(shard[None], (peers, *shard.shape)), axis...  11.5 us
    dot_general x2, matrix products, contract_rows(): lax.dot_general(left, right, (((0,), (0,)), ((), ())), preferred_element_...  10.8 us
    concatenate x1, other arithmetic, on_device(): jnp.concatenate([contract_rows(whole_tokens, gate_grad), contract_rows(wh...  10.7 us
  transfers between devices with their start and end apart: 12, of which 10 were waited for; matrix products, arithmetic and copies ran while one was open for 21% of the time, Pallas kernels for 0%

profile of v1, /device:TPU:8, one launch (start us, length us, event | category | flops | bytes accessed | tf_op | source)
XLA Modules:
  0.0 276.5 jit_solution(14638624689193232796)
XLA Ops:
  8.1 1.7 pad_maximum_fusion.1
  9.9 8.8 %collective-permute-done = bf16[128,2048]{1,0:T(8,128)(2,1)S(1)} collective-permute-done((bf16[128,2048]{1,0:T(8,128)(2,1)}, bf16[128,2048]{1,0:T(8,128)(2,1)S(1)}, u32[]{:S(2)}, u32[]{:S(2)}) %collective-permute-start) | collective-permute-done | bytes 524320 | tf_op jit(solution)/shard_map/ppermute | solution.py:74
  18.7 8.6 %collective-permute-done.1 = bf16[128,2048]{1,0:T(8,128)(2,1)S(1)} collective-permute-done((bf16[128,2048]{1,0:T(8,128)(2,1)S(1)}, bf16[128,2048]{1,0:T(8,128)(2,1)S(1)}, u32[]{:S(2)}, u32[]{:S(2)}) %collective-permute-start.1) | collective-permute-done | bytes 524320 | tf_op jit(solution)/shard_map/ppermute | solution.py:74
  27.3 8.6 %collective-permute-done.2 = bf16[128,2048]{1,0:T(8,128)(2,1)S(1)} collective-permute-done((bf16[128,2048]{1,0:T(8,128)(2,1)S(1)}, bf16[128,2048]{1,0:T(8,128)(2,1)S(1)}, u32[]{:S(2)}, u32[]{:S(2)}) %collective-permute-start.2) | collective-permute-done | bytes 524320 | tf_op jit(solution)/shard_map/ppermute | solution.py:74
  35.9 8.6 %collective-permute-done.3 = bf16[128,2048]{1,0:T(8,128)(2,1)S(1)} collective-permute-done((bf16[128,2048]{1,0:T(8,128)(2,1)S(1)}, bf16[128,2048]{1,0:T(8,128)(2,1)S(1)}, u32[]{:S(2)}, u32[]{:S(2)}) %collective-permute-start.3) | collective-permute-done | bytes 524320 | tf_op jit(solution)/shard_map/ppermute | solution.py:74
  44.5 8.6 %collective-permute-done.4 = bf16[128,2048]{1,0:T(8,128)(2,1)S(1)} collective-permute-done((bf16[128,2048]{1,0:T(8,128)(2,1)S(1)}, bf16[128,2048]{1,0:T(8,128)(2,1)S(1)}, u32[]{:S(2)}, u32[]{:S(2)}) %collective-permute-start.4) | collective-permute-done | bytes 524320 | tf_op jit(solution)/shard_map/ppermute | solution.py:74
  53.2 1.9 convert_element_type.26
  55.2 6.7 %collective-permute-done.5 = bf16[128,2048]{1,0:T(8,128)(2,1)} collective-permute-done((bf16[128,2048]{1,0:T(8,128)(2,1)S(1)}, bf16[128,2048]{1,0:T(8,128)(2,1)}, u32[]{:S(2)}, u32[]{:S(2)}) %collective-permute-start.5) | collective-permute-done | bytes 524320 | tf_op jit(solution)/shard_map/ppermute | solution.py:74
  61.9 6.5 %multiply_reduce_fusion.2 = (f32[704]{0:T(1024)S(1)}, f32[704]{0:T(1024)S(1)}, f32[704]{0:T(1024)S(1)}, f32[704]{0:T(1024)S(1)}, f32[1024,704]{0,1:T(8,128)S(1)}, /*index=5*/f32[1024,704]{0,1:T(8,128)}) fusion(f32[1024,704]{0,1:T(8,128)S(1)} %convert_element_type.26, bf16[1024,704]{0,1:T(8,128)(2,1)S(1)} %copy-done, bf16[1024,704]{0,1:T(8,128)(2,1)S(1)} %copy-done.11, ...), kind=kLoop, calls=%fused_computation.31 | loop fusion | flops 25949440 | bytes 12998656 | tf_op jit(solution)/shard_map/reduce_sum | solution.py:103
  68.5 2.1 fusion.10
  70.6 0.3 collective-permute-done.6
  70.8 1.7 constant_dynamic-update-slice_fusion.15
  72.5 1.2 constant_dynamic-update-slice_fusion.14
  74.0 1.1 constant_dynamic-update-slice_fusion.7
  75.1 1.1 constant_dynamic-update-slice_fusion.6
  76.5 5.0 %fusion = f32[2048,704]{0,1:T(8,128)} fusion(bf16[1024,704]{0,1:T(8,128)(2,1)S(1)} %fusion.10, bf16[2048,2048]{1,0:T(8,128)(2,1)S(1)} %constant_dynamic-update-slice_fusion, s32[]{:T(128)S(6)} %select_n.14), kind=kOutput, calls=%fused_computation.4 | convolution fusion | flops 2952790016 | bytes 11403268 | tf_op jit(solution)/shard_map/dot_general | solution.py:51
  81.4 5.9 %fusion.2 = f32[2048,704]{0,1:T(8,128)} fusion(bf16[2048,2048]{1,0:T(8,128)(2,1)S(1)} %constant_dynamic-update-slice_fusion, s32[]{:T(128)S(6)} %select_n.14, bf16[1024,704]{0,1:T(8,128)(2,1)S(1)} %copy-done.13, f32[1024,704]{0,1:T(8,128)S(1)} %copy-done.1), kind=kOutput, calls=%fused_computation.6 | convolution fusion | flops 2960719872 | bytes 14286852 | tf_op jit(solution)/shard_map/dot_general | solution.py:51
  87.3 10.7 %pad_maximum_fusion = f32[2048,1408]{0,1:T(8,128)} fusion(f32[2048,704]{0,1:T(8,128)} %fusion.2, f32[2048,704]{0,1:T(8,128)} %fusion), kind=kLoop, calls=%fused_computation | loop fusion | flops 2883584 | bytes 23068672 | tf_op jit(solution)/shard_map/concatenate | solution.py:113
  98.1 0.8 broadcast_in_dim.2
  98.9 11.5 %all-to-all-start.1 = ((f32[32,4,704]{2,1,0:T(4,128)}), f32[32,4,704]{2,1,0:T(4,128)S(1)}, u32[]{:S(2)}, u32[]{:S(2)}) async-start(f32[32,4,704]{2,1,0:T(4,128)} %broadcast_in_dim.2), calls=%async_computation.2 | async-start | bytes 786432 | tf_op jit(solution)/shard_map/all_to_all | solution.py:14
  110.4 6.0 %fusion.5 = f32[1024,2048]{1,0:T(8,128)S(1)} fusion(bf16[1024,704]{0,1:T(8,128)(2,1)} %copy-done.15, bf16[2048,1408]{1,0:T(8,128)(2,1)} %all-gather.2.cloned.1.call-done), kind=kOutput, calls=%fused_computation.15 | convolution fusion | flops 2952790016 | bytes 12976128 | tf_op jit(solution)/shard_map/dot_general | solution.py:57
  116.5 7.6 %add_convert_fusion = bf16[1024,2048]{1,0:T(8,128)(2,1)} fusion(f32[1024,2048]{1,0:T(8,128)S(1)} %fusion.5, bf16[2048,1408]{1,0:T(8,128)(2,1)S(1)} %copy-done.19, bf16[1024,704]{0,1:T(8,128)(2,1)S(1)} %copy-done.14, f32[1024,704]{0,1:T(8,128)S(1)} %copy-done.1), kind=kOutput, calls=%fused_computation.1 | convolution fusion | flops 2964914176 | bytes 20054016 | tf_op jit(solution)/shard_map/dot_general | solution.py:57
  124.0 2.3 all-to-all-done.1
  126.3 13.0 %all-to-all-start = ((bf16[8,128,2048]{2,1,0:T(8,128)(2,1)}), bf16[8,128,2048]{2,1,0:T(8,128)(2,1)}, u32[]{:S(2)}, u32[]{:S(2)}) async-start(bf16[8,128,2048]{2,1,0:T(8,128)(2,1)} %bitcast.5), calls=%async_computation | async-start | bytes 8388608 | tf_op jit(solution)/shard_map/all_to_all | solution.py:46
  139.4 94.0 %reduce-scatter.5.cloned.1.call-done = f32[256,1408]{0,1:T(8,128)} async-done(((f32[2048,1408]{0,1:T(8,128)}), f32[256,1408]{0,1:T(8,128)}) %reduce-scatter.5.cloned.1.call-update) | async-done | bytes 1441808 | tf_op jit(solution)/shard_map/reduce_scatter | solution.py:34
  233.3 2.9 %copy.22 = f32[256,1408]{1,0:T(8,128)} copy(f32[256,1408]{0,1:T(8,128)} %reduce-scatter.5.cloned.1.call-done) | data formatting | bytes 2883584
  236.4 0.6 slice_reduce_fusion
  237.0 3.8 %reduce_sum.57 = bf16[128,2048]{1,0:T(8,128)(2,1)} reduce(bf16[8,128,2048]{2,1,0:T(8,128)(2,1)} %all-to-all-done, bf16[]{:T(256)} %constant.42.clone.1), dimensions={0}, to_apply=%region_0.1 | reduce | flops 1835008 | bytes 4718594 | tf_op jit(solution)/shard_map/reduce_sum | solution.py:47
  240.8 25.0 %reduce-scatter.7.cloned.1.call-done = f32[64,1408]{1,0:T(8,128)} async-done(((f32[256,1408]{1,0:T(8,128)}), f32[64,1408]{1,0:T(8,128)}) %reduce-scatter.7.cloned.1.call-update) | async-done | bytes 360464
  265.8 1.1 fusion.24
  267.2 0.8 copy.20
  268.2 0.8 copy.21
  (79 shorter events, 1.3 us)
Async XLA Ops:
  8.0 47.1 %copy-start.17 = (f32[3,704]{1,0:T(4,128)S(1)}, f32[3,704]{1,0:T(4,128)}, u32[]{:S(2)}) copy-start(f32[3,704]{1,0:T(4,128)} %param.13) | copy-start | bytes 25348
  8.0 53.9 %copy-start.18 = (f32[704]{0:T(1024)S(1)}, f32[704]{0:T(1024)}, u32[]{:S(2)}) copy-start(f32[704]{0:T(1024)} %param.14) | copy-start | bytes 8452
  8.0 102.4 %all-gather.2.cloned.1.call-start = ((), (), s32[]{:S(2)}) async-start(), calls=%async_computation.4 | async-start | bytes 5947392 | tf_op jit(solution)/shard_map/all_gather | solution.py:29
  9.8 223.5 %reduce-scatter.5.cloned.1.call-start = ((), (), s32[]{:S(2)}) async-start(), calls=%async_computation.5 | async-start | bytes 12976128 | tf_op jit(solution)/shard_map/reduce_scatter | solution.py:34
  9.9 52.1 %copy-start = (bf16[1024,704]{0,1:T(8,128)(2,1)S(1)}, bf16[1024,704]{0,1:T(8,128)(2,1)}, u32[]{:S(2)}) copy-start(bf16[1024,704]{0,1:T(8,128)(2,1)} %param.9) | copy-start | bytes 4325380
  9.9 52.1 %copy-start.11 = (bf16[1024,704]{0,1:T(8,128)(2,1)S(1)}, bf16[1024,704]{0,1:T(8,128)(2,1)}, u32[]{:S(2)}) copy-start(bf16[1024,704]{0,1:T(8,128)(2,1)} %param.10) | copy-start | bytes 4325380
  9.9 52.1 %copy-start.12 = (bf16[1024,704]{0,1:T(8,128)(2,1)S(1)}, bf16[1024,704]{0,1:T(8,128)(2,1)}, u32[]{:S(2)}) copy-start(bf16[1024,704]{0,1:T(8,128)(2,1)} %param.15) | copy-start | bytes 4325380
  9.9 8.8 %collective-permute-start = (bf16[128,2048]{1,0:T(8,128)(2,1)}, bf16[128,2048]{1,0:T(8,128)(2,1)S(1)}, u32[]{:S(2)}, u32[]{:S(2)}) collective-permute-start(bf16[128,2048]{1,0:T(8,128)(2,1)} %param.8), channel_id=1, source_target_pairs={{0,1},{1,2},{2,3},{3,4},{4,5},{5,6},{6,7},{7,0},{8,9},{9,10},{10,1... | collective-permute-start | bytes 1572872 | tf_op jit(solution)/shard_map/ppermute | solution.py:74
  18.7 8.6 %collective-permute-start.1 = (bf16[128,2048]{1,0:T(8,128)(2,1)S(1)}, bf16[128,2048]{1,0:T(8,128)(2,1)S(1)}, u32[]{:S(2)}, u32[]{:S(2)}) collective-permute-start(bf16[128,2048]{1,0:T(8,128)(2,1)S(1)} %collective-permute-done), channel_id=1, source_target_pairs={{0,1},{1,2},{2,3},{3,4},{4,5},{5,6},{6,7},{7,0},{8,9},{9,10},{10,1... | collective-permute-start | bytes 1572872 | tf_op jit(solution)/shard_map/ppermute | solution.py:74
  27.3 25.8 %copy-start.3 = (bf16[128,2048]{1,0:T(8,128)(2,1)}, bf16[128,2048]{1,0:T(8,128)(2,1)S(1)}, u32[]{:S(2)}) copy-start(bf16[128,2048]{1,0:T(8,128)(2,1)S(1)} %collective-permute-done.1) | copy-start | bytes 1572868
  27.3 8.6 %collective-permute-start.2 = (bf16[128,2048]{1,0:T(8,128)(2,1)S(1)}, bf16[128,2048]{1,0:T(8,128)(2,1)S(1)}, u32[]{:S(2)}, u32[]{:S(2)}) collective-permute-start(bf16[128,2048]{1,0:T(8,128)(2,1)S(1)} %collective-permute-done.1), channel_id=1, source_target_pairs={{0,1},{1,2},{2,3},{3,4},{4,5},{5,6},{6,7},{7,0},{8,9},{9,10},{10,1... | collective-permute-start | bytes 1572872 | tf_op jit(solution)/shard_map/ppermute | solution.py:74
  35.9 17.2 %copy-start.5 = (bf16[128,2048]{1,0:T(8,128)(2,1)}, bf16[128,2048]{1,0:T(8,128)(2,1)S(1)}, u32[]{:S(2)}) copy-start(bf16[128,2048]{1,0:T(8,128)(2,1)S(1)} %collective-permute-done.2) | copy-start | bytes 1572868
  35.9 8.6 %collective-permute-start.3 = (bf16[128,2048]{1,0:T(8,128)(2,1)S(1)}, bf16[128,2048]{1,0:T(8,128)(2,1)S(1)}, u32[]{:S(2)}, u32[]{:S(2)}) collective-permute-start(bf16[128,2048]{1,0:T(8,128)(2,1)S(1)} %collective-permute-done.2), channel_id=1, source_target_pairs={{0,1},{1,2},{2,3},{3,4},{4,5},{5,6},{6,7},{7,0},{8,9},{9,10},{10,1... | collective-permute-start | bytes 1572872 | tf_op jit(solution)/shard_map/ppermute | solution.py:74
  44.5 8.6 %copy-start.7 = (bf16[128,2048]{1,0:T(8,128)(2,1)}, bf16[128,2048]{1,0:T(8,128)(2,1)S(1)}, u32[]{:S(2)}) copy-start(bf16[128,2048]{1,0:T(8,128)(2,1)S(1)} %collective-permute-done.3) | copy-start | bytes 1572868
  44.5 8.6 %collective-permute-start.4 = (bf16[128,2048]{1,0:T(8,128)(2,1)S(1)}, bf16[128,2048]{1,0:T(8,128)(2,1)S(1)}, u32[]{:S(2)}, u32[]{:S(2)}) collective-permute-start(bf16[128,2048]{1,0:T(8,128)(2,1)S(1)} %collective-permute-done.3), channel_id=1, source_target_pairs={{0,1},{1,2},{2,3},{3,4},{4,5},{5,6},{6,7},{7,0},{8,9},{9,10},{10,1... | collective-permute-start | bytes 1572872 | tf_op jit(solution)/shard_map/ppermute | solution.py:74
  53.2 8.7 %copy-start.9 = (bf16[128,2048]{1,0:T(8,128)(2,1)}, bf16[128,2048]{1,0:T(8,128)(2,1)S(1)}, u32[]{:S(2)}) copy-start(bf16[128,2048]{1,0:T(8,128)(2,1)S(1)} %collective-permute-done.4) | copy-start | bytes 1572868
  53.2 8.7 %collective-permute-start.5 = (bf16[128,2048]{1,0:T(8,128)(2,1)S(1)}, bf16[128,2048]{1,0:T(8,128)(2,1)}, u32[]{:S(2)}, u32[]{:S(2)}) collective-permute-start(bf16[128,2048]{1,0:T(8,128)(2,1)S(1)} %collective-permute-done.4), channel_id=1, source_target_pairs={{0,1},{1,2},{2,3},{3,4},{4,5},{5,6},{6,7},{7,0},{8,9},{9,10},{10,1... | collective-permute-start | bytes 1572872 | tf_op jit(solution)/shard_map/ppermute | solution.py:74
  61.9 8.9 %collective-permute-start.6 = (bf16[128,2048]{1,0:T(8,128)(2,1)}, bf16[128,2048]{1,0:T(8,128)(2,1)}, u32[]{:S(2)}, u32[]{:S(2)}) collective-permute-start(bf16[128,2048]{1,0:T(8,128)(2,1)} %collective-permute-done.5), channel_id=1, source_target_pairs={{0,1},{1,2},{2,3},{3,4},{4,5},{5,6},{6,7},{7,0},{8,9},{9,10},{10,1... | collective-permute-start | bytes 1572872 | tf_op jit(solution)/shard_map/ppermute | solution.py:74
  68.5 5.2 %copy-start.10 = (bf16[128,2048]{1,0:T(8,128)(2,1)S(1)}, bf16[128,2048]{1,0:T(8,128)(2,1)}, u32[]{:S(2)}) copy-start(bf16[128,2048]{1,0:T(8,128)(2,1)} %copy-done.9) | copy-start | bytes 1572868
  68.5 5.3 %copy-start.8 = (bf16[128,2048]{1,0:T(8,128)(2,1)S(1)}, bf16[128,2048]{1,0:T(8,128)(2,1)}, u32[]{:S(2)}) copy-start(bf16[128,2048]{1,0:T(8,128)(2,1)} %copy-done.7) | copy-start | bytes 1572868
  70.5 5.9 %copy-start.15 = (bf16[1024,704]{0,1:T(8,128)(2,1)}, bf16[1024,704]{0,1:T(8,128)(2,1)S(1)}, u32[]{:S(2)}) copy-start(bf16[1024,704]{0,1:T(8,128)(2,1)S(1)} %fusion.10) | copy-start | bytes 4325380
  70.5 3.2 %copy-start.6 = (bf16[128,2048]{1,0:T(8,128)(2,1)S(1)}, bf16[128,2048]{1,0:T(8,128)(2,1)}, u32[]{:S(2)}) copy-start(bf16[128,2048]{1,0:T(8,128)(2,1)} %copy-done.5) | copy-start | bytes 1572868
  70.5 3.3 %copy-start.4 = (bf16[128,2048]{1,0:T(8,128)(2,1)S(1)}, bf16[128,2048]{1,0:T(8,128)(2,1)}, u32[]{:S(2)}) copy-start(bf16[128,2048]{1,0:T(8,128)(2,1)} %copy-done.3) | copy-start | bytes 1572868
  72.5 1.4 copy-start.2
  76.4 5.0 %copy-start.1 = (f32[1024,704]{0,1:T(8,128)S(1)}, f32[1024,704]{0,1:T(8,128)}, u32[]{:S(2)}) copy-start(f32[1024,704]{0,1:T(8,128)} %get-tuple-element.33) | copy-start | bytes 8650756
  76.5 5.0 %copy-start.13 = (bf16[1024,704]{0,1:T(8,128)(2,1)S(1)}, bf16[1024,704]{0,1:T(8,128)(2,1)}, u32[]{:S(2)}) copy-start(bf16[1024,704]{0,1:T(8,128)(2,1)} %param.15) | copy-start | bytes 4325380
  98.9 27.5 %all-to-all-start.1 = ((f32[32,4,704]{2,1,0:T(4,128)}), f32[32,4,704]{2,1,0:T(4,128)S(1)}, u32[]{:S(2)}, u32[]{:S(2)}) async-start(f32[32,4,704]{2,1,0:T(4,128)} %broadcast_in_dim.2), calls=%async_computation.2 | async-start | bytes 786432 | tf_op jit(solution)/shard_map/all_to_all | solution.py:14
  110.4 6.0 %copy-start.14 = (bf16[1024,704]{0,1:T(8,128)(2,1)S(1)}, bf16[1024,704]{0,1:T(8,128)(2,1)}, u32[]{:S(2)}) copy-start(bf16[1024,704]{0,1:T(8,128)(2,1)} %param.15) | copy-start | bytes 4325380
  110.4 6.0 %copy-start.19 = (bf16[2048,1408]{1,0:T(8,128)(2,1)S(1)}, bf16[2048,1408]{1,0:T(8,128)(2,1)}, u32[]{:S(2)}) copy-start(bf16[2048,1408]{1,0:T(8,128)(2,1)} %all-gather.2.cloned.1.call-done) | copy-start | bytes 17301508
  126.3 110.6 %all-to-all-start = ((bf16[8,128,2048]{2,1,0:T(8,128)(2,1)}), bf16[8,128,2048]{2,1,0:T(8,128)(2,1)}, u32[]{:S(2)}, u32[]{:S(2)}) async-start(bf16[8,128,2048]{2,1,0:T(8,128)(2,1)} %bitcast.5), calls=%async_computation | async-start | bytes 8388608 | tf_op jit(solution)/shard_map/all_to_all | solution.py:46
  139.4 126.4 %reduce-scatter.7.cloned.1.call-start = ((), (), s32[]{:S(2)}) async-start(), calls=%async_computation.6 | async-start | bytes 1802240
  236.4 30.8 %copy-start.16 = (f32[4,704]{1,0:T(4,128)}, f32[4,704]{1,0:T(4,128)S(1)}, u32[]{:S(2)}) copy-start(f32[4,704]{1,0:T(4,128)S(1)} %broadcast_multiply_fusion.2) | copy-start | bytes 33796
Sparse Core Ops, SparseCore 0:
  12.0 89.4 all-gather.1
Sparse Core Ops, SparseCore 1:
  98.1 135.2 reduce-scatter.4
  236.4 29.4 reduce-scatter.6
